TPU v7x, 32 devices: a whole 2x2x4 slice. The times are simulated.
32 devices in a mesh: sp: 16 (over z, y, x), tp: 2 (over core).
Axes of the slice: x: 2, y: 2, z: 4, core: 2. Of those that a mesh axis runs over, the one named last changes fastest.
Arguments:
- residual: bfloat16 [3072, 2048], P(('sp', 'tp')), may hold values from -6 to 6
- queries: bfloat16 [3072, 1024], P('sp', 'tp'), may hold values from -6 to 6
- key_pairs: bfloat16 [3072, 1024], P('sp', 'tp'), may hold values from -6 to 6
- values: bfloat16 [3072, 1024], P('sp', 'tp'), may hold values from -6 to 6
- second_weight: float32 [8], P('tp'), may hold values from 0.3 to 0.8
- head_gain: float32 [1024], P('tp'), may hold values from 0.1 to 1.9
- out_weight: bfloat16 [1024, 2048], P('tp'), may hold values from -0.1875 to 0.1875
- norm_gain: float32 [2048], replicated, may hold values from 0.1 to 1.9
- up_weight: bfloat16 [2048, 5632], P('sp', 'tp'), may hold values from -0.125 to 0.125
- gate_weight: bfloat16 [2048, 5632], P('sp', 'tp'), may hold values from -0.125 to 0.125
- conv_weight: float32 [3, 5632], P(None, 'tp'), may hold values from -3.5 to 3.5
- conv_bias: float32 [5632], P('tp'), may hold values from -3 to 3
- down_weight: bfloat16 [5632, 2048], P('tp', 'sp'), may hold values from -0.078125 to 0.078125
Outputs:
- layer_out: bfloat16 [3072, 2048], P(('sp', 'tp'))
All inputs are finite; a program needn't handle non-finite values.
Results may differ from a plain program's by a relative error of at most 0.017.
Values may be sent and summed in bfloat16 or wider, within the bound.
A program may use at most 128 MiB of HBM per device.

v0:
```python
import jax
import jax.numpy as jnp
from jax import lax
from jax.sharding import PartitionSpec as P

HD = 64
VD = 128
eps = 1e-05
neg_fill = -1e30


def from_behind(value, axis, steps):
    count = lax.axis_size(axis)
    leading, last = (max(0, -steps), min(count, count - steps))
    return lax.ppermute(value, axis, [(source, source + steps) for source in range(leading, last)])


def normalize(rows_in, gain):
    values_f = rows_in.astype(jnp.float32)
    scale_inv = lax.rsqrt(jnp.mean(values_f * values_f, axis=-1, keepdims=True) + eps)
    return (values_f * scale_inv * gain).astype(jnp.bfloat16)


def local(
    residual,
    queries,
    key_pairs,
    values,
    second_weight,
    head_gain,
    out_weight,
    norm_gain,
    up_weight,
    gate_weight,
    conv_weight,
    conv_bias,
    down_weight,
):
    tok_rows = queries.shape[0]
    head_count = second_weight.shape[0]
    ff_local = up_weight.shape[1]
    sp_index = lax.axis_index("sp")
    query = queries.reshape(tok_rows, head_count, 2, HD)
    query_pos = sp_index * tok_rows + jnp.arange(tok_rows)
    last_query = (sp_index + 1) * tok_rows
    initial = (
        jnp.full((head_count, 2, tok_rows), neg_fill, jnp.float32),
        jnp.zeros((head_count, 2, tok_rows), jnp.float32),
        jnp.zeros((head_count, 2, tok_rows, VD), jnp.float32),
    )
    key_piece = lax.all_gather(key_pairs, "sp", axis=0, tiled=True)
    value_piece = lax.all_gather(values, "sp", axis=0, tiled=True)
    piece_len = key_piece.shape[0]

    def compute(state_in):
        maxima, totals, weighted = state_in
        key_rows = key_piece.reshape(piece_len, head_count, 2, HD)
        value_rows = value_piece.reshape(piece_len, head_count, VD)
        scores = jnp.einsum(
            "qhmd,khmd->hmqk", query, key_rows, preferred_element_type=jnp.float32
        ) * HD ** (-0.5)
        visible = jnp.arange(piece_len)[None, :] <= query_pos[:, None]
        scores = jnp.where(visible, scores, neg_fill)
        new_max = jnp.maximum(maxima, jnp.max(scores, axis=-1))
        exp_scores = jnp.where(visible, jnp.exp(scores - new_max[..., None]), jnp.float32(0.0))
        totals = jnp.sum(exp_scores, axis=-1)
        weighted = jnp.einsum(
            "hmqk,khe->hmqe",
            exp_scores.astype(jnp.bfloat16),
            value_rows,
            preferred_element_type=jnp.float32,
        )
        return (new_max, totals, weighted)

    def keep_state(state_in):
        return state_in

    maxima, totals, weighted = lax.cond(jnp.int32(0) < last_query, compute, keep_state, initial)
    diff = (
        weighted[:, 0] / totals[:, 0, :, None]
        - second_weight[:, None, None] * weighted[:, 1] / totals[:, 1, :, None]
    )
    diff = jnp.transpose(diff, (1, 0, 2))
    scale_inv = lax.rsqrt(jnp.mean(diff * diff, axis=-1, keepdims=True) + eps)
    attended = (
        (diff * scale_inv * head_gain.reshape(head_count, VD) * 0.8)
        .reshape(tok_rows, head_count * VD)
        .astype(jnp.bfloat16)
    )
    proj = lax.psum_scatter(
        jnp.dot(attended, out_weight, preferred_element_type=jnp.float32).astype(jnp.bfloat16),
        "tp",
        scatter_dimension=0,
        tiled=True,
    )
    mid = (residual.astype(jnp.float32) + proj.astype(jnp.float32)).astype(jnp.bfloat16)
    normed_all = lax.all_gather(normalize(mid, norm_gain), "tp", axis=0, tiled=True)
    up_sum = jnp.dot(
        normed_all,
        lax.all_gather(up_weight, "sp", axis=0, tiled=True),
        preferred_element_type=jnp.float32,
    )
    gate_sum = jnp.dot(
        normed_all,
        lax.all_gather(gate_weight, "sp", axis=0, tiled=True),
        preferred_element_type=jnp.float32,
    )
    up_proj = up_sum.astype(jnp.bfloat16)
    gate_proj = gate_sum.astype(jnp.bfloat16)
    taps = conv_weight.shape[0]
    rim_rows = from_behind(up_proj[tok_rows - (taps - 1) :], "sp", 1)
    extended = jnp.concatenate((rim_rows, up_proj), axis=0)
    conv_out = jnp.zeros((tok_rows, ff_local), jnp.float32) + conv_bias[None, :]
    for tap in range(taps):
        conv_out = conv_out + conv_weight[tap][None, :] * extended[tap : tap + tok_rows].astype(
            jnp.float32
        )
    hidden = (jax.nn.silu(conv_out) * gate_proj.astype(jnp.float32)).astype(jnp.bfloat16)
    down_all = lax.all_gather(down_weight, "sp", axis=1, tiled=True)
    ffn_out = lax.psum_scatter(
        jnp.dot(hidden, down_all, preferred_element_type=jnp.float32).astype(jnp.bfloat16),
        "tp",
        scatter_dimension=0,
        tiled=True,
    )
    return (mid.astype(jnp.float32) + ffn_out.astype(jnp.float32)).astype(jnp.bfloat16)


def solution(mesh):
    return jax.shard_map(
        local,
        mesh=mesh,
        in_specs=(
            P(("sp", "tp"), None),
            P("sp", "tp"),
            P("sp", "tp"),
            P("sp", "tp"),
            P("tp"),
            P("tp"),
            P("tp", None),
            P(),
            P("sp", "tp"),
            P("sp", "tp"),
            P(None, "tp"),
            P("tp"),
            P("tp", "sp"),
        ),
        out_specs=P(("sp", "tp"), None),
        check_vma=False,
    )
```

profile of v0, /device:TPU:0, one launch (start us, length us, event | category | flops | bytes accessed | tf_op | source)
XLA Modules:
  0.0 705.0 jit_solution(9887044699763358971)
XLA Ops:
  6.5 0.7 all-gather.6.cloned.1.call-update
  7.3 0.7 all-gather.8.cloned.1.call-update
  8.0 0.0 reduce-scatter.3.cloned.1.call-start
  8.1 72.7 %all-gather.6.cloned.1.call-done = bf16[3072,512]{1,0:T(8,128)(2,1)} async-done(((bf16[192,512]{1,0:T(8,128)(2,1)}), bf16[3072,512]{1,0:T(8,128)(2,1)}) %all-gather.6.cloned.1.call-update) | async-done | bytes 3145744 | tf_op jit(solution)/shard_map/all_gather | solution.py:51
  80.7 69.2 %all-gather.8.cloned.1.call-done = bf16[3072,512]{1,0:T(8,128)(2,1)} async-done(((bf16[192,512]{1,0:T(8,128)(2,1)}), bf16[3072,512]{1,0:T(8,128)(2,1)}) %all-gather.8.cloned.1.call-update) | async-done | bytes 3145744 | tf_op jit(solution)/shard_map/all_gather | solution.py:52
  150.0 45.3 %conditional.1 = (f32[4,2,192]{2,1,0:T(2,128)S(1)}, f32[4,2,192,128]{3,2,1,0:T(8,128)S(1)}) conditional(s32[]{:T(128)} %convert_element_type.62, () %tuple.13, (s32[]{:T(128)}, s32[192]{0:T(256)S(1)}, bf16[192,512]{1,0:T(8,128)(2,1)}, bf16[3072,512]{1,0:T(8,128)(2,1)}, bf16[3072,512]{1,0:T(8,128)(2,1)}) %tuple.14), branch_computations={%region_0.0_spmd, %region_1.4_spmd} | conditional | flops 1873869568 | bytes 80058688 | solution.py:78
  150.0 0.4 iota_compare_fusion
  150.4 4.8 copy.26
  155.2 0.1 copy.25
  155.3 11.8 %fusion = (f32[4,2,192]{2,1,0:T(2,128)S(1)}, f32[4,2,192,3072]{3,2,1,0:T(8,128)}) fusion(pred[192,3072]{1,0:T(8,128)(4,1)S(1)} %iota_compare_fusion, bf16[192,4,2,64]{0,3,2,1:T(8,128)(2,1)S(1)} %bitcast.44, bf16[3072,4,2,64]{0,3,2,1:T(8,128)(2,1)} %bitcast.42), kind=kOutput, calls=%fused_computation.2 | convolution fusion | flops 618134016 | bytes 22812672 | tf_op jit(solution)/shard_map/cond/branch_1_fun/qhmd,khmd->hmqk/dot_general | solution.py:59
  167.1 5.5 reshape.37
  172.6 10.7 %fusion.3 = f32[4,2,192,128]{3,2,1,0:T(8,128)S(1)} fusion(f32[4,2,192,3072]{3,2,1,0:T(8,128)} %get-tuple-element.52, f32[4,2,192]{2,1,0:T(2,128)S(1)} %broadcast_maximum_fusion, pred[192,3072]{1,0:T(8,128)(4,1)S(1)} %iota_compare_fusion, bf16[3072,4,128,1]{2,1,0,3:T(4,128)(2,1)} %bitcast.43), kind=kOutput, calls=%fused_computation.5 | convolution fusion | flops 1231552512 | bytes 23402496 | tf_op jit(solution)/shard_map/cond/branch_1_fun/hmqk,khe->hmqe/dot_general | solution.py:67
  183.3 11.9 %fusion.2 = f32[4,2,192]{2,1,0:T(2,128)S(1)} fusion(f32[4,2,192,3072]{3,2,1,0:T(8,128)} %get-tuple-element.52, f32[4,2,192]{2,1,0:T(2,128)S(1)} %broadcast_maximum_fusion, pred[192,3072]{1,0:T(8,128)(4,1)S(1)} %iota_compare_fusion), kind=kLoop, calls=%fused_computation.4 | loop fusion | flops 23591424 | bytes 19476480 | tf_op jit(solution)/shard_map/cond/branch_1_fun/reduce_sum | solution.py:66
  195.3 0.5 multiply_reduce_fusion
  195.8 1.5 convolution_convert_fusion.3
  197.4 0.0 all-gather.10.cloned.1.call-start
  197.4 0.5 all-gather.10.cloned.1.call-update
  198.0 0.5 all-gather.12.cloned.1.call-update
  198.6 0.5 all-gather.14.cloned.1.call-update
  199.1 5.1 reduce-scatter.3.cloned.1.call-done
  204.2 1.2 fusion.20
  205.5 1.2 fusion.22
  206.6 2.4 all_gather.20
  209.0 140.4 %all-gather.10.cloned.1.call-done = bf16[2048,2816]{1,0:T(8,128)(2,1)} async-done(((bf16[128,2816]{1,0:T(8,128)(2,1)}), bf16[2048,2816]{1,0:T(8,128)(2,1)}) %all-gather.10.cloned.1.call-update) | async-done | bytes 11534352 | tf_op jit(solution)/shard_map/all_gather | solution.py:100
  349.4 6.7 convolution_convert_fusion.1
  356.1 3.4 collective-permute-start
  359.5 0.1 slice_reduce_fusion.2
  359.6 132.0 %all-gather.12.cloned.1.call-done = bf16[2048,2816]{1,0:T(8,128)(2,1)} async-done(((bf16[128,2816]{1,0:T(8,128)(2,1)}), bf16[2048,2816]{1,0:T(8,128)(2,1)}) %all-gather.12.cloned.1.call-update) | async-done | bytes 11534352 | tf_op jit(solution)/shard_map/all_gather | solution.py:105
  491.6 182.8 %all-gather.14.cloned.1.call-done = bf16[2816,2048]{1,0:T(8,128)(2,1)} async-done(((bf16[2816,128]{1,0:T(8,128)(2,1)}), bf16[2816,2048]{1,0:T(8,128)(2,1)}) %all-gather.14.cloned.1.call-update) | async-done | bytes 11534352 | tf_op jit(solution)/shard_map/all_gather | solution.py:119
  674.5 15.2 %convolution_convert_fusion.2 = bf16[192,2048]{1,0:T(8,128)(2,1)} fusion(bf16[2816,2048]{1,0:T(8,128)(2,1)} %all-gather.14.cloned.1.call-done, bf16[192,2048]{1,0:T(8,128)(2,1)} %copy-done.4, bf16[2048,2816]{1,0:T(8,128)(2,1)} %all-gather.12.cloned.1.call-done, bf16[192,2816]{1,0:T(8,128)(2,1)} %copy-done.10, bf16[2,2816]{1,0:T(2,128)(2,1)S(1)} %collective-permute-done, ...), kind=kOutput, calls=%fused_computation.19 | convolution fusion | flops 4442013696 | bytes 25779200 | tf_op jit(solution)/shard_map/dot_general | solution.py:121
  689.7 6.5 reduce-scatter.5.cloned.1.call-done
  696.2 1.9 fusion.23
  (40 shorter events, 0.3 us)
Async XLA Ops:
  6.5 189.2 %copy-start = (bf16[512,2048]{1,0:T(8,128)(2,1)S(1)}, bf16[512,2048]{1,0:T(8,128)(2,1)}, u32[]{:S(2)}) copy-start(bf16[512,2048]{1,0:T(8,128)(2,1)} %param.21) | copy-start | bytes 6291460
  6.5 74.2 %all-gather.6.cloned.1.call-start = ((), (), s32[]{:S(2)}) async-start(), calls=%async_computation.2 | async-start | bytes 3342336 | tf_op jit(solution)/shard_map/all_gather | solution.py:51
  7.3 142.7 %all-gather.8.cloned.1.call-start = ((), (), s32[]{:S(2)}) async-start(), calls=%async_computation.3 | async-start | bytes 3342336 | tf_op jit(solution)/shard_map/all_gather | solution.py:52
  8.0 196.2 %reduce-scatter.3.cloned.1.call-start = ((), (), s32[]{:S(2)}) async-start(), calls=%async_computation.4 | async-start | bytes 1179648 | tf_op jit(solution)/shard_map/reduce_scatter | solution.py:90
  149.9 45.3 %copy-start.9 = (f32[4]{0:T(128)S(1)}, f32[4]{0:T(128)}, u32[]{:S(2)}) copy-start(f32[4]{0:T(128)} %param.19) | copy-start | bytes 52
  149.9 45.8 %copy-start.8 = (f32[512]{0:T(512)S(1)}, f32[512]{0:T(512)}, u32[]{:S(2)}) copy-start(f32[512]{0:T(512)} %param.20) | copy-start | bytes 6148
  150.3 4.8 copy-start.5
  195.7 8.5 %copy-start.2 = (bf16[96,2048]{1,0:T(8,128)(2,1)S(1)}, bf16[96,2048]{1,0:T(8,128)(2,1)}, u32[]{:S(2)}) copy-start(bf16[96,2048]{1,0:T(8,128)(2,1)} %param.15) | copy-start | bytes 1179652
  195.8 9.7 %copy-start.7 = (f32[2048]{0:T(1024)S(1)}, f32[2048]{0:T(1024)}, u32[]{:S(2)}) copy-start(f32[2048]{0:T(1024)} %param.22) | copy-start | bytes 24580
  197.4 152.0 %all-gather.10.cloned.1.call-start = ((), (), s32[]{:S(2)}) async-start(), calls=%async_computation.5 | async-start | bytes 12255232 | tf_op jit(solution)/shard_map/all_gather | solution.py:100
  197.9 293.7 %all-gather.12.cloned.1.call-start = ((), (), s32[]{:S(2)}) async-start(), calls=%async_computation.6 | async-start | bytes 12255232 | tf_op jit(solution)/shard_map/all_gather | solution.py:105
  198.5 475.9 %all-gather.14.cloned.1.call-start = ((), (), s32[]{:S(2)}) async-start(), calls=%async_computation.7 | async-start | bytes 12255232 | tf_op jit(solution)/shard_map/all_gather | solution.py:119
  199.1 497.1 %reduce-scatter.5.cloned.1.call-start = ((), (), s32[]{:S(2)}) async-start(), calls=%async_computation.8 | async-start | bytes 1179648 | tf_op jit(solution)/shard_map/reduce_scatter | solution.py:120
  209.0 147.1 %copy-start.4 = (bf16[192,2048]{1,0:T(8,128)(2,1)}, bf16[192,2048]{1,0:T(8,128)(2,1)S(1)}, u32[]{:S(2)}) copy-start(bf16[192,2048]{1,0:T(8,128)(2,1)S(1)} %all_gather.20) | copy-start | bytes 2359300
  209.0 150.5 %copy-start.6 = (f32[3,2816]{1,0:T(4,128)S(1)}, f32[3,2816]{1,0:T(4,128)}, u32[]{:S(2)}) copy-start(f32[3,2816]{1,0:T(4,128)} %param.25) | copy-start | bytes 101380
  209.0 465.5 %copy-start.11 = (f32[2816]{0:T(1024)S(1)}, f32[2816]{0:T(1024)}, u32[]{:S(2)}) copy-start(f32[2816]{0:T(1024)} %param.26) | copy-start | bytes 33796
  356.1 3.4 copy-start.10
  356.1 318.3 %collective-permute-start = (bf16[2,2816]{1,0:T(2,128)(2,1)S(1)}, bf16[2,2816]{1,0:T(2,128)(2,1)S(1)}, u32[]{:S(2)}, u32[]{:S(2)}) collective-permute-start(bf16[2,2816]{1,0:T(2,128)(2,1)S(1)} %slice.41), channel_id=1, source_target_pairs={{0,2},{2,4},{4,6},{6,8},{8,10},{10,12},{12,14},{14,16},{16,18},{18... | collective-permute-start | bytes 33800 | tf_op jit(solution)/shard_map/ppermute | solution.py:15
  674.5 21.8 %copy-start.3 = (bf16[96,2048]{1,0:T(8,128)(2,1)S(1)}, bf16[96,2048]{1,0:T(8,128)(2,1)}, u32[]{:S(2)}) copy-start(bf16[96,2048]{1,0:T(8,128)(2,1)} %reduce-scatter.3.cloned.1.call-done) | copy-start | bytes 1179652
  674.5 23.7 %copy-start.1 = (bf16[512,2048]{1,0:T(8,128)(2,1)S(1)}, bf16[512,2048]{1,0:T(8,128)(2,1)}, u32[]{:S(2)}) copy-start(bf16[512,2048]{1,0:T(8,128)(2,1)} %param.21) | copy-start | bytes 6291460
Sparse Core Ops, SparseCore 0:
  10.1 70.5 all-gather.5
  83.5 66.3 all-gather.7
  197.5 6.6 reduce-scatter.2
  206.8 142.5 all-gather.9
  352.0 139.5 all-gather.11
  494.2 180.2 all-gather.13
  689.8 6.3 reduce-scatter.4
where the time goes:
time: 706 us; the launch traced here: 705 us
  waiting for transfers between devices  612 us (87%)
  matrix products  45.9 us (7%)
  other arithmetic  17.1 us (2%)
  between operations  13.6 us (2%)
  local copies, waits for them, and re-layouts  10.6 us (2%)
    all_gather x1, waiting for transfers between devices, local(): down_all = lax.all_gather(down_weight, 'sp', axis=1, tiled=True)  183 us
    all_gather x1, waiting for transfers between devices, local(): lax.all_gather(up_weight, 'sp', axis=0, tiled=True)  140 us
    all_gather x1, waiting for transfers between devices, local(): lax.all_gather(gate_weight, 'sp', axis=0, tiled=True)  132 us
    all_gather x1, waiting for transfers between devices, local(): key_piece = lax.all_gather(key_pairs, 'sp', axis=0, tiled=True)  72.7 us
    all_gather x1, waiting for transfers between devices, local(): value_piece = lax.all_gather(values, 'sp', axis=0, tiled=True)  69.2 us
    dot_general x1, matrix products, local(): jnp.dot(hidden, down_all, preferred_element_type=jnp.float32)  15.2 us
  transfers between devices with their start and end apart: 8, of which 7 were waited for; matrix products, arithmetic and copies ran while one was open for 1% of the time, Pallas kernels for 0%

commit v1 on v0

--- a/solution.py
+++ b/solution.py
@@ -116,7 +116,12 @@
             jnp.float32
         )
     hidden = (jax.nn.silu(conv_out) * gate_proj.astype(jnp.float32)).astype(jnp.bfloat16)
-    down_all = lax.all_gather(down_weight, "sp", axis=1, tiled=True)
+    ring = [down_weight]
+    for hop in range(15):
+        ring.append(lax.ppermute(ring[-1], "sp", [(dev, (dev + 1) % 16) for dev in range(16)]))
+    down_all = jnp.roll(
+        jnp.concatenate(ring[::-1], axis=1), (lax.axis_index("sp") + 1) * ring[0].shape[1], axis=1
+    )
     ffn_out = lax.psum_scatter(
         jnp.dot(hidden, down_all, preferred_element_type=jnp.float32).astype(jnp.bfloat16),
         "tp",

time: 706 us -> 762 us (1.079)
  local copies, waits for them, and re-layouts: 10.6 us -> 68.6 us
    ppermute x0 -> x15, waiting for transfers between devices: none -> 457 us  [local(): lax.ppermute(ring[-1], 'sp', [(dev, (dev + 1) % 16) for dev in range(16)])]
    all_gather x1 -> x0, waiting for transfers between devices: 183 us -> none  [local(): down_all = lax.all_gather(down_weight, 'sp', axis=1, tiled=True)]
    all_gather x1, waiting for transfers between devices: 140 us -> 0.01 us  [local(): lax.all_gather(up_weight, 'sp', axis=0, tiled=True)]
    all_gather x1, waiting for transfers between devices: 132 us -> 0.01 us  [local(): lax.all_gather(gate_weight, 'sp', axis=0, tiled=True)]
    unnamed x23 -> x92, local copies, waits for them, and re-layouts: 0.05 us -> 56.3 us
  transfers between devices with their start and end apart: 8 -> 22, of which waited for: 7 -> 19; matrix products, arithmetic and copies ran while one was open for 1% -> 8% of each run, Pallas kernels for 0% -> 0%
where the time goes in v1:
time: 762 us; the launch traced here: 761 us
  waiting for transfers between devices  608 us (80%)
  local copies, waits for them, and re-layouts  68.6 us (9%)
  matrix products  46.7 us (6%)
  other arithmetic  18.4 us (2%)
  between operations  13.7 us (2%)
    ppermute x15, waiting for transfers between devices, local(): lax.ppermute(ring[-1], 'sp', [(dev, (dev + 1) % 16) for dev in range(16)])  457 us
    all_gather x1, waiting for transfers between devices, local(): key_piece = lax.all_gather(key_pairs, 'sp', axis=0, tiled=True)  72.7 us
    all_gather x1, waiting for transfers between devices, local(): value_piece = lax.all_gather(values, 'sp', axis=0, tiled=True)  69.2 us
    unnamed x92, local copies, waits for them, and re-layouts  56.3 us
  transfers between devices with their start and end apart: 22, of which 19 were waited for; matrix products, arithmetic and copies ran while one was open for 8% of the time, Pallas kernels for 0%

profile of v1, /device:TPU:0, one launch (start us, length us, event | category | flops | bytes accessed | tf_op | source)
XLA Modules:
  0.0 761.1 jit_solution(5334766728992978369)
XLA Ops:
  8.1 72.7 %all-gather.5.cloned.1.call-done = bf16[3072,512]{1,0:T(8,128)(2,1)} async-done(((bf16[192,512]{1,0:T(8,128)(2,1)}), bf16[3072,512]{1,0:T(8,128)(2,1)}) %all-gather.5.cloned.1.call-update) | async-done | bytes 3145744 | tf_op jit(solution)/shard_map/all_gather | solution.py:51
  80.7 69.2 %all-gather.7.cloned.1.call-done = bf16[3072,512]{1,0:T(8,128)(2,1)} async-done(((bf16[192,512]{1,0:T(8,128)(2,1)}), bf16[3072,512]{1,0:T(8,128)(2,1)}) %all-gather.7.cloned.1.call-update) | async-done | bytes 3145744 | tf_op jit(solution)/shard_map/all_gather | solution.py:52
  150.0 46.6 %conditional.1 = (f32[4,2,192]{2,1,0:T(2,128)S(1)}, f32[4,2,192,128]{3,2,1,0:T(8,128)}) conditional(s32[]{:T(128)} %convert_element_type.62, () %tuple.13, (s32[]{:T(128)}, s32[192]{0:T(256)S(1)}, bf16[192,512]{1,0:T(8,128)(2,1)}, bf16[3072,512]{1,0:T(8,128)(2,1)}, bf16[3072,512]{1,0:T(8,128)(2,1)}) %tuple.14), branch_computations={%region_0.0_spmd, %region_1.4_spmd} | conditional | flops 1873869568 | bytes 79272224 | solution.py:78
  150.4 4.7 copy.26
  156.1 11.8 %fusion = (f32[4,2,192]{2,1,0:T(2,128)S(1)}, f32[4,2,192,3072]{3,2,1,0:T(8,128)}) fusion(pred[192,3072]{1,0:T(8,128)(4,1)S(1)} %iota_compare_fusion, bf16[192,4,2,64]{0,3,2,1:T(8,128)(2,1)S(1)} %bitcast.43, bf16[3072,4,2,64]{0,3,2,1:T(8,128)(2,1)} %bitcast.41), kind=kOutput, calls=%fused_computation.2 | convolution fusion | flops 618134016 | bytes 22812672 | tf_op jit(solution)/shard_map/cond/branch_1_fun/qhmd,khmd->hmqk/dot_general | solution.py:59
  167.9 5.5 reshape.37
  173.4 11.3 %fusion.3 = f32[4,2,192,128]{3,2,1,0:T(8,128)} fusion(f32[4,2,192,3072]{3,2,1,0:T(8,128)} %get-tuple-element.52, f32[4,2,192]{2,1,0:T(2,128)S(1)} %broadcast_maximum_fusion, pred[192,3072]{1,0:T(8,128)(4,1)S(1)} %iota_compare_fusion, bf16[3072,4,128,1]{2,1,0,3:T(4,128)(2,1)} %bitcast.42), kind=kOutput, calls=%fused_computation.5 | convolution fusion | flops 1231552512 | bytes 23402496 | tf_op jit(solution)/shard_map/cond/branch_1_fun/hmqk,khe->hmqe/dot_general | solution.py:67
  184.7 11.9 %fusion.2 = f32[4,2,192]{2,1,0:T(2,128)S(1)} fusion(f32[4,2,192,3072]{3,2,1,0:T(8,128)} %get-tuple-element.52, f32[4,2,192]{2,1,0:T(2,128)S(1)} %broadcast_maximum_fusion, pred[192,3072]{1,0:T(8,128)(4,1)S(1)} %iota_compare_fusion), kind=kLoop, calls=%fused_computation.4 | loop fusion | flops 23591424 | bytes 19476480 | tf_op jit(solution)/shard_map/cond/branch_1_fun/reduce_sum | solution.py:66
  202.1 18.3 %collective-permute-done.1 = bf16[2816,128]{1,0:T(8,128)(2,1)S(1)} collective-permute-done((bf16[2816,128]{1,0:T(8,128)(2,1)}, bf16[2816,128]{1,0:T(8,128)(2,1)S(1)}, u32[]{:S(2)}, u32[]{:S(2)}) %collective-permute-start.1) | collective-permute-done | bytes 720928 | tf_op jit(solution)/shard_map/ppermute | solution.py:121
  221.2 34.3 %collective-permute-done.2 = bf16[2816,128]{1,0:T(8,128)(2,1)} collective-permute-done((bf16[2816,128]{1,0:T(8,128)(2,1)S(1)}, bf16[2816,128]{1,0:T(8,128)(2,1)}, u32[]{:S(2)}, u32[]{:S(2)}) %collective-permute-start.2) | collective-permute-done | bytes 720928 | tf_op jit(solution)/shard_map/ppermute | solution.py:121
  255.6 35.9 %collective-permute-done.3 = bf16[2816,128]{1,0:T(8,128)(2,1)} collective-permute-done((bf16[2816,128]{1,0:T(8,128)(2,1)}, bf16[2816,128]{1,0:T(8,128)(2,1)}, u32[]{:S(2)}, u32[]{:S(2)}) %collective-permute-start.3) | collective-permute-done | bytes 720928 | tf_op jit(solution)/shard_map/ppermute | solution.py:121
  291.5 30.9 %collective-permute-done.4 = bf16[2816,128]{1,0:T(8,128)(2,1)S(1)} collective-permute-done((bf16[2816,128]{1,0:T(8,128)(2,1)}, bf16[2816,128]{1,0:T(8,128)(2,1)S(1)}, u32[]{:S(2)}, u32[]{:S(2)}) %collective-permute-start.4) | collective-permute-done | bytes 720928 | tf_op jit(solution)/shard_map/ppermute | solution.py:121
  323.3 37.0 %collective-permute-done.5 = bf16[2816,128]{1,0:T(8,128)(2,1)S(1)} collective-permute-done((bf16[2816,128]{1,0:T(8,128)(2,1)S(1)}, bf16[2816,128]{1,0:T(8,128)(2,1)S(1)}, u32[]{:S(2)}, u32[]{:S(2)}) %collective-permute-start.5) | collective-permute-done | bytes 720928 | tf_op jit(solution)/shard_map/ppermute | solution.py:121
  361.2 37.5 %collective-permute-done.6 = bf16[2816,128]{1,0:T(8,128)(2,1)S(1)} collective-permute-done((bf16[2816,128]{1,0:T(8,128)(2,1)S(1)}, bf16[2816,128]{1,0:T(8,128)(2,1)S(1)}, u32[]{:S(2)}, u32[]{:S(2)}) %collective-permute-start.6) | collective-permute-done | bytes 720928 | tf_op jit(solution)/shard_map/ppermute | solution.py:121
  399.6 34.5 %collective-permute-done.7 = bf16[2816,128]{1,0:T(8,128)(2,1)S(1)} collective-permute-done((bf16[2816,128]{1,0:T(8,128)(2,1)S(1)}, bf16[2816,128]{1,0:T(8,128)(2,1)S(1)}, u32[]{:S(2)}, u32[]{:S(2)}) %collective-permute-start.7) | collective-permute-done | bytes 720928 | tf_op jit(solution)/shard_map/ppermute | solution.py:121
  435.0 29.3 %collective-permute-done.8 = bf16[2816,128]{1,0:T(8,128)(2,1)S(1)} collective-permute-done((bf16[2816,128]{1,0:T(8,128)(2,1)S(1)}, bf16[2816,128]{1,0:T(8,128)(2,1)S(1)}, u32[]{:S(2)}, u32[]{:S(2)}) %collective-permute-start.8) | collective-permute-done | bytes 720928 | tf_op jit(solution)/shard_map/ppermute | solution.py:121
  465.1 26.7 %collective-permute-done.9 = bf16[2816,128]{1,0:T(8,128)(2,1)S(1)} collective-permute-done((bf16[2816,128]{1,0:T(8,128)(2,1)S(1)}, bf16[2816,128]{1,0:T(8,128)(2,1)S(1)}, u32[]{:S(2)}, u32[]{:S(2)}) %collective-permute-start.9) | collective-permute-done | bytes 720928 | tf_op jit(solution)/shard_map/ppermute | solution.py:121
  492.7 36.4 %collective-permute-done.10 = bf16[2816,128]{1,0:T(8,128)(2,1)S(1)} collective-permute-done((bf16[2816,128]{1,0:T(8,128)(2,1)S(1)}, bf16[2816,128]{1,0:T(8,128)(2,1)S(1)}, u32[]{:S(2)}, u32[]{:S(2)}) %collective-permute-start.10) | collective-permute-done | bytes 720928 | tf_op jit(solution)/shard_map/ppermute | solution.py:121
  530.0 25.9 %collective-permute-done.11 = bf16[2816,128]{1,0:T(8,128)(2,1)S(1)} collective-permute-done((bf16[2816,128]{1,0:T(8,128)(2,1)S(1)}, bf16[2816,128]{1,0:T(8,128)(2,1)S(1)}, u32[]{:S(2)}, u32[]{:S(2)}) %collective-permute-start.11) | collective-permute-done | bytes 720928 | tf_op jit(solution)/shard_map/ppermute | solution.py:121
  556.7 35.9 %collective-permute-done.12 = bf16[2816,128]{1,0:T(8,128)(2,1)S(1)} collective-permute-done((bf16[2816,128]{1,0:T(8,128)(2,1)S(1)}, bf16[2816,128]{1,0:T(8,128)(2,1)S(1)}, u32[]{:S(2)}, u32[]{:S(2)}) %collective-permute-start.12) | collective-permute-done | bytes 720928 | tf_op jit(solution)/shard_map/ppermute | solution.py:121
  593.4 35.9 %collective-permute-done.13 = bf16[2816,128]{1,0:T(8,128)(2,1)} collective-permute-done((bf16[2816,128]{1,0:T(8,128)(2,1)S(1)}, bf16[2816,128]{1,0:T(8,128)(2,1)}, u32[]{:S(2)}, u32[]{:S(2)}) %collective-permute-start.13) | collective-permute-done | bytes 720928 | tf_op jit(solution)/shard_map/ppermute | solution.py:121
  631.0 26.9 %collective-permute-done.14 = bf16[2816,128]{1,0:T(8,128)(2,1)} collective-permute-done((bf16[2816,128]{1,0:T(8,128)(2,1)}, bf16[2816,128]{1,0:T(8,128)(2,1)}, u32[]{:S(2)}, u32[]{:S(2)}) %collective-permute-start.14) | collective-permute-done | bytes 720928 | tf_op jit(solution)/shard_map/ppermute | solution.py:121
  659.1 2.9 all_gather.17
  662.0 11.1 %collective-permute-done.15 = bf16[2816,128]{1,0:T(8,128)(2,1)S(1)} collective-permute-done((bf16[2816,128]{1,0:T(8,128)(2,1)}, bf16[2816,128]{1,0:T(8,128)(2,1)S(1)}, u32[]{:S(2)}, u32[]{:S(2)}) %collective-permute-start.15) | collective-permute-done | bytes 720928 | tf_op jit(solution)/shard_map/ppermute | solution.py:121
  680.2 2.1 constant_dynamic-update-slice_fusion.27
  686.4 2.1 constant_dynamic-update-slice_fusion.24
  690.6 2.1 constant_dynamic-update-slice_fusion.22
  692.7 2.1 constant_dynamic-update-slice_fusion.21
  697.8 2.1 constant_dynamic-update-slice_fusion.18
  720.7 6.9 convolution_convert_fusion.1
  730.4 15.1 %fusion.15 = bf16[192,2048]{1,0:T(8,128)(2,1)} fusion(bf16[2816,4096]{1,0:T(8,128)(2,1)} %constant_dynamic-update-slice_fusion, s32[]{:T(128)S(6)} %select_n.22, bf16[192,2048]{1,0:T(8,128)(2,1)} %all_gather.17, bf16[2048,2816]{1,0:T(8,128)(2,1)} %all-gather.11.cloned.1.call-done, bf16[192,2816]{1,0:T(8,128)(2,1)} %copy-done.28, ...), kind=kOutput, calls=%fused_computation.21 | convolution fusion | flops 4442013696 | bytes 25779204 | tf_op jit(solution)/shard_map/dot_general | solution.py:126
  745.5 6.9 reduce-scatter.5.cloned.1.call-done
  (135 shorter events, 61.4 us)
Async XLA Ops:
  6.5 191.8 %copy-start = (bf16[512,2048]{1,0:T(8,128)(2,1)S(1)}, bf16[512,2048]{1,0:T(8,128)(2,1)}, u32[]{:S(2)}) copy-start(bf16[512,2048]{1,0:T(8,128)(2,1)} %param.21) | copy-start | bytes 6291460
  6.5 74.2 %all-gather.5.cloned.1.call-start = ((), (), s32[]{:S(2)}) async-start(), calls=%async_computation.2 | async-start | bytes 3342336 | tf_op jit(solution)/shard_map/all_gather | solution.py:51
  7.3 142.7 %all-gather.7.cloned.1.call-start = ((), (), s32[]{:S(2)}) async-start(), calls=%async_computation.3 | async-start | bytes 3342336 | tf_op jit(solution)/shard_map/all_gather | solution.py:52
  8.0 621.5 %reduce-scatter.3.cloned.1.call-start = ((), (), s32[]{:S(2)}) async-start(), calls=%async_computation.4 | async-start | bytes 1179648 | tf_op jit(solution)/shard_map/reduce_scatter | solution.py:90
  150.0 479.4 %copy-start.24 = (f32[3,2816]{1,0:T(4,128)S(1)}, f32[3,2816]{1,0:T(4,128)}, u32[]{:S(2)}) copy-start(f32[3,2816]{1,0:T(4,128)} %param.25) | copy-start | bytes 101380
  150.0 479.6 %copy-start.1 = (bf16[96,2048]{1,0:T(8,128)(2,1)S(1)}, bf16[96,2048]{1,0:T(8,128)(2,1)}, u32[]{:S(2)}) copy-start(bf16[96,2048]{1,0:T(8,128)(2,1)} %param.15) | copy-start | bytes 1179652
  150.0 508.0 %copy-start.25 = (f32[2048]{0:T(1024)S(1)}, f32[2048]{0:T(1024)}, u32[]{:S(2)}) copy-start(f32[2048]{0:T(1024)} %param.22) | copy-start | bytes 24580
  196.6 504.2 %copy-start.3 = (bf16[2816,128]{1,0:T(8,128)(2,1)S(1)}, bf16[2816,128]{1,0:T(8,128)(2,1)}, u32[]{:S(2)}) copy-start(bf16[2816,128]{1,0:T(8,128)(2,1)} %param.27) | copy-start | bytes 2162692
  199.9 520.8 %all-gather.9.cloned.1.call-start = ((), (), s32[]{:S(2)}) async-start(), calls=%async_computation.5 | async-start | bytes 12255232 | tf_op jit(solution)/shard_map/all_gather | solution.py:100
  200.5 529.5 %all-gather.11.cloned.1.call-start = ((), (), s32[]{:S(2)}) async-start(), calls=%async_computation.6 | async-start | bytes 12255232 | tf_op jit(solution)/shard_map/all_gather | solution.py:105
  200.5 19.8 %collective-permute-start.1 = (bf16[2816,128]{1,0:T(8,128)(2,1)}, bf16[2816,128]{1,0:T(8,128)(2,1)S(1)}, u32[]{:S(2)}, u32[]{:S(2)}) collective-permute-start(bf16[2816,128]{1,0:T(8,128)(2,1)} %param.27), channel_id=1, source_target_pairs={{0,2},{2,4},{4,6},{6,8},{8,10},{10,12},{12,14},{14,16},{16,18},{18... | collective-permute-start | bytes 2162696 | tf_op jit(solution)/shard_map/ppermute | solution.py:121
  221.2 34.3 %collective-permute-start.2 = (bf16[2816,128]{1,0:T(8,128)(2,1)S(1)}, bf16[2816,128]{1,0:T(8,128)(2,1)}, u32[]{:S(2)}, u32[]{:S(2)}) collective-permute-start(bf16[2816,128]{1,0:T(8,128)(2,1)S(1)} %collective-permute-done.1), channel_id=1, source_target_pairs={{0,2},{2,4},{4,6},{6,8},{8,10},{10,12},{12,14},{14,16},{16,18},{18... | collective-permute-start | bytes 2162696 | tf_op jit(solution)/shard_map/ppermute | solution.py:121
  255.5 36.0 %collective-permute-start.3 = (bf16[2816,128]{1,0:T(8,128)(2,1)}, bf16[2816,128]{1,0:T(8,128)(2,1)}, u32[]{:S(2)}, u32[]{:S(2)}) collective-permute-start(bf16[2816,128]{1,0:T(8,128)(2,1)} %collective-permute-done.2), channel_id=1, source_target_pairs={{0,2},{2,4},{4,6},{6,8},{8,10},{10,12},{12,14},{14,16},{16,18},{18... | collective-permute-start | bytes 2162696 | tf_op jit(solution)/shard_map/ppermute | solution.py:121
  255.5 496.9 %reduce-scatter.5.cloned.1.call-start = ((), (), s32[]{:S(2)}) async-start(), calls=%async_computation.7 | async-start | bytes 1179648 | tf_op jit(solution)/shard_map/reduce_scatter | solution.py:125
  291.5 30.9 %collective-permute-start.4 = (bf16[2816,128]{1,0:T(8,128)(2,1)}, bf16[2816,128]{1,0:T(8,128)(2,1)S(1)}, u32[]{:S(2)}, u32[]{:S(2)}) collective-permute-start(bf16[2816,128]{1,0:T(8,128)(2,1)} %collective-permute-done.3), channel_id=1, source_target_pairs={{0,2},{2,4},{4,6},{6,8},{8,10},{10,12},{12,14},{14,16},{16,18},{18... | collective-permute-start | bytes 2162696 | tf_op jit(solution)/shard_map/ppermute | solution.py:121
  323.3 37.0 %collective-permute-start.5 = (bf16[2816,128]{1,0:T(8,128)(2,1)S(1)}, bf16[2816,128]{1,0:T(8,128)(2,1)S(1)}, u32[]{:S(2)}, u32[]{:S(2)}) collective-permute-start(bf16[2816,128]{1,0:T(8,128)(2,1)S(1)} %collective-permute-done.4), channel_id=1, source_target_pairs={{0,2},{2,4},{4,6},{6,8},{8,10},{10,12},{12,14},{14,16},{16,18},{18... | collective-permute-start | bytes 2162696 | tf_op jit(solution)/shard_map/ppermute | solution.py:121
  361.2 37.5 %collective-permute-start.6 = (bf16[2816,128]{1,0:T(8,128)(2,1)S(1)}, bf16[2816,128]{1,0:T(8,128)(2,1)S(1)}, u32[]{:S(2)}, u32[]{:S(2)}) collective-permute-start(bf16[2816,128]{1,0:T(8,128)(2,1)S(1)} %collective-permute-done.5), channel_id=1, source_target_pairs={{0,2},{2,4},{4,6},{6,8},{8,10},{10,12},{12,14},{14,16},{16,18},{18... | collective-permute-start | bytes 2162696 | tf_op jit(solution)/shard_map/ppermute | solution.py:121
  399.6 34.5 %collective-permute-start.7 = (bf16[2816,128]{1,0:T(8,128)(2,1)S(1)}, bf16[2816,128]{1,0:T(8,128)(2,1)S(1)}, u32[]{:S(2)}, u32[]{:S(2)}) collective-permute-start(bf16[2816,128]{1,0:T(8,128)(2,1)S(1)} %collective-permute-done.6), channel_id=1, source_target_pairs={{0,2},{2,4},{4,6},{6,8},{8,10},{10,12},{12,14},{14,16},{16,18},{18... | collective-permute-start | bytes 2162696 | tf_op jit(solution)/shard_map/ppermute | solution.py:121
  435.0 29.3 %collective-permute-start.8 = (bf16[2816,128]{1,0:T(8,128)(2,1)S(1)}, bf16[2816,128]{1,0:T(8,128)(2,1)S(1)}, u32[]{:S(2)}, u32[]{:S(2)}) collective-permute-start(bf16[2816,128]{1,0:T(8,128)(2,1)S(1)} %collective-permute-done.7), channel_id=1, source_target_pairs={{0,2},{2,4},{4,6},{6,8},{8,10},{10,12},{12,14},{14,16},{16,18},{18... | collective-permute-start | bytes 2162696 | tf_op jit(solution)/shard_map/ppermute | solution.py:121
  465.1 26.7 %collective-permute-start.9 = (bf16[2816,128]{1,0:T(8,128)(2,1)S(1)}, bf16[2816,128]{1,0:T(8,128)(2,1)S(1)}, u32[]{:S(2)}, u32[]{:S(2)}) collective-permute-start(bf16[2816,128]{1,0:T(8,128)(2,1)S(1)} %collective-permute-done.8), channel_id=1, source_target_pairs={{0,2},{2,4},{4,6},{6,8},{8,10},{10,12},{12,14},{14,16},{16,18},{18... | collective-permute-start | bytes 2162696 | tf_op jit(solution)/shard_map/ppermute | solution.py:121
  492.6 36.4 %collective-permute-start.10 = (bf16[2816,128]{1,0:T(8,128)(2,1)S(1)}, bf16[2816,128]{1,0:T(8,128)(2,1)S(1)}, u32[]{:S(2)}, u32[]{:S(2)}) collective-permute-start(bf16[2816,128]{1,0:T(8,128)(2,1)S(1)} %collective-permute-done.9), channel_id=1, source_target_pairs={{0,2},{2,4},{4,6},{6,8},{8,10},{10,12},{12,14},{14,16},{16,18},{18... | collective-permute-start | bytes 2162696 | tf_op jit(solution)/shard_map/ppermute | solution.py:121
  530.0 25.9 %collective-permute-start.11 = (bf16[2816,128]{1,0:T(8,128)(2,1)S(1)}, bf16[2816,128]{1,0:T(8,128)(2,1)S(1)}, u32[]{:S(2)}, u32[]{:S(2)}) collective-permute-start(bf16[2816,128]{1,0:T(8,128)(2,1)S(1)} %collective-permute-done.10), channel_id=1, source_target_pairs={{0,2},{2,4},{4,6},{6,8},{8,10},{10,12},{12,14},{14,16},{16,18},{18... | collective-permute-start | bytes 2162696 | tf_op jit(solution)/shard_map/ppermute | solution.py:121
  556.7 35.9 %collective-permute-start.12 = (bf16[2816,128]{1,0:T(8,128)(2,1)S(1)}, bf16[2816,128]{1,0:T(8,128)(2,1)S(1)}, u32[]{:S(2)}, u32[]{:S(2)}) collective-permute-start(bf16[2816,128]{1,0:T(8,128)(2,1)S(1)} %collective-permute-done.11), channel_id=1, source_target_pairs={{0,2},{2,4},{4,6},{6,8},{8,10},{10,12},{12,14},{14,16},{16,18},{18... | collective-permute-start | bytes 2162696 | tf_op jit(solution)/shard_map/ppermute | solution.py:121
  593.4 36.0 %collective-permute-start.13 = (bf16[2816,128]{1,0:T(8,128)(2,1)S(1)}, bf16[2816,128]{1,0:T(8,128)(2,1)}, u32[]{:S(2)}, u32[]{:S(2)}) collective-permute-start(bf16[2816,128]{1,0:T(8,128)(2,1)S(1)} %collective-permute-done.12), channel_id=1, source_target_pairs={{0,2},{2,4},{4,6},{6,8},{8,10},{10,12},{12,14},{14,16},{16,18},{18... | collective-permute-start | bytes 2162696 | tf_op jit(solution)/shard_map/ppermute | solution.py:121
  629.4 28.5 %collective-permute-start.14 = (bf16[2816,128]{1,0:T(8,128)(2,1)}, bf16[2816,128]{1,0:T(8,128)(2,1)}, u32[]{:S(2)}, u32[]{:S(2)}) collective-permute-start(bf16[2816,128]{1,0:T(8,128)(2,1)} %collective-permute-done.13), channel_id=1, source_target_pairs={{0,2},{2,4},{4,6},{6,8},{8,10},{10,12},{12,14},{14,16},{16,18},{18... | collective-permute-start | bytes 2162696 | tf_op jit(solution)/shard_map/ppermute | solution.py:121
  629.6 78.4 %copy-start.21 = (bf16[2816,128]{1,0:T(8,128)(2,1)S(1)}, bf16[2816,128]{1,0:T(8,128)(2,1)}, u32[]{:S(2)}) copy-start(bf16[2816,128]{1,0:T(8,128)(2,1)} %copy-done.20) | copy-start | bytes 2162692
  629.6 79.3 %copy-start.19 = (bf16[2816,128]{1,0:T(8,128)(2,1)S(1)}, bf16[2816,128]{1,0:T(8,128)(2,1)}, u32[]{:S(2)}) copy-start(bf16[2816,128]{1,0:T(8,128)(2,1)} %copy-done.18) | copy-start | bytes 2162692
  629.6 80.3 %copy-start.17 = (bf16[2816,128]{1,0:T(8,128)(2,1)S(1)}, bf16[2816,128]{1,0:T(8,128)(2,1)}, u32[]{:S(2)}) copy-start(bf16[2816,128]{1,0:T(8,128)(2,1)} %copy-done.16) | copy-start | bytes 2162692
  629.6 81.2 %copy-start.15 = (bf16[2816,128]{1,0:T(8,128)(2,1)S(1)}, bf16[2816,128]{1,0:T(8,128)(2,1)}, u32[]{:S(2)}) copy-start(bf16[2816,128]{1,0:T(8,128)(2,1)} %copy-done.14) | copy-start | bytes 2162692
  629.6 82.2 %copy-start.13 = (bf16[2816,128]{1,0:T(8,128)(2,1)S(1)}, bf16[2816,128]{1,0:T(8,128)(2,1)}, u32[]{:S(2)}) copy-start(bf16[2816,128]{1,0:T(8,128)(2,1)} %copy-done.12) | copy-start | bytes 2162692
  657.9 15.1 %collective-permute-start.15 = (bf16[2816,128]{1,0:T(8,128)(2,1)}, bf16[2816,128]{1,0:T(8,128)(2,1)S(1)}, u32[]{:S(2)}, u32[]{:S(2)}) collective-permute-start(bf16[2816,128]{1,0:T(8,128)(2,1)} %collective-permute-done.14), channel_id=1, source_target_pairs={{0,2},{2,4},{4,6},{6,8},{8,10},{10,12},{12,14},{14,16},{16,18},{18... | collective-permute-start | bytes 2162696 | tf_op jit(solution)/shard_map/ppermute | solution.py:121
  727.7 2.7 collective-permute-start
  (20 other events, 467.8 us)
Sparse Core Ops, SparseCore 0:
  10.1 70.5 all-gather.4
  83.5 66.3 all-gather.6
  200.0 6.6 reduce-scatter.2
  209.4 208.3 all-gather.8
  420.4 219.7 all-gather.10
  745.7 6.6 reduce-scatter.4
